TPU v7x, 256 devices: a whole 4x4x8 slice. The times are simulated.
256 devices in a mesh: sp: 64 (over z, x, core), tp: 4 (over y).
Axes of the slice: x: 4, y: 4, z: 8, core: 2. Of those that a mesh axis runs over, the one named last changes fastest.
Arguments:
- residual_in: bfloat16 [16384, 2048], P('sp', 'tp'), may hold values from -6 to 6
- conv_input: bfloat16 [16384, 512], P('sp', 'tp'), may hold values from -6 to 6
- outer_gate: bfloat16 [16384, 512], P('sp', 'tp'), may hold values from -6 to 6
- inner_gate: bfloat16 [16384, 512], P('sp', 'tp'), may hold values from -6 to 6
- documents: int32 [16384], P('sp'), may hold values from 0 to 31, as said below
- conv_taps: float32 [3, 512], P(None, 'tp'), may hold values from -3 to 3
- mixer_gain: float32 [512], replicated, may hold values from 0.1 to 1.9
- output_weight: bfloat16 [512, 2048], P(None, 'tp'), may hold values from -0.25 to 0.25
- ffn_gain: float32 [2048], P('tp'), may hold values from 0.1 to 1.9
- routes: int32 [16384, 2], P('sp'), may hold values from 0 to 63, all different within a row; in each aligned block of 256 rows (0 to 255, 256 to 511, ...) at most 16 rows name the same one
- route_weights: float32 [16384, 2], P('sp'), may hold values from 0.1 to 0.9
- expert_gate: bfloat16 [64, 2048, 3584], P('sp', None, 'tp'), may hold values from -0.125 to 0.125
- expert_up: bfloat16 [64, 2048, 3584], P('sp', None, 'tp'), may hold values from -0.125 to 0.125
- expert_down: bfloat16 [64, 3584, 2048], P('sp', 'tp'), may hold values from -0.09375 to 0.09375
Outputs:
- layer_out: bfloat16 [16384, 2048], P('sp', 'tp')
Inputs may be any that keep to these rules, and one draw needn't show every extreme that they name: Document numbers never fall along the positions, and each of the 32 documents occurs. Every document has 256 to 768 positions, and one has exactly 768. `routes`: the two experts of a position differ. Among the 256 positions of one index of sp no expert is named more than 16 times, a bound that some block reaches.
All inputs are finite; a program needn't handle non-finite values.
Results may differ from a plain program's by a relative error of at most 0.0058.
Values may be sent and summed in bfloat16 or wider, within the bound.
A program may use at most 64 MiB of HBM per device.

v0:
```python
import jax
import jax.numpy as jnp
from jax import lax
from jax.sharding import PartitionSpec as P

EPS = 1e-06


def from_behind(block, axis, distance):
    devices = range(lax.axis_size(axis))
    route = [(i - distance, i) for i in devices if i - distance in devices]
    return lax.ppermute(block, axis, route)


def laid_out(pieces, dim):
    dims = list(pieces.shape[1:])
    dims[dim] *= pieces.shape[0]
    return jnp.moveaxis(pieces, 0, dim).reshape(dims)


def sent_to_all(shard, axis):
    copies = jnp.broadcast_to(shard, (lax.axis_size(axis), *shard.shape))
    return lax.all_to_all(copies, axis, split_axis=0, concat_axis=0, tiled=True)


def gather_directly(shard, axis, dim):
    return laid_out(sent_to_all(shard, axis), dim)


def over_copies(shard, axis):
    return sent_to_all(shard, axis).sum(axis=0)


def slot_tables(routes, experts, capacity):
    tokens = routes.shape[0]
    flattened = routes.reshape(-1)
    onehot = (flattened[:, None] == jnp.arange(experts, dtype=jnp.int32)[None, :]).astype(jnp.int32)
    earlier = jnp.cumsum(onehot, axis=0) - onehot
    position_in = jnp.sum(earlier * onehot, axis=1)
    target = flattened * capacity + position_in
    owners = (
        jnp.full((experts * capacity,), tokens, jnp.int32)
        .at[target]
        .set(jnp.arange(2 * tokens, dtype=jnp.int32) // 2)
    )
    return (target, owners)


def per_device(
    residual_in,
    conv_input,
    outer_gate,
    inner_gate,
    documents,
    conv_taps,
    mixer_gain,
    output_weight,
    ffn_gain,
    routes,
    route_weights,
    expert_gate,
    expert_up,
    expert_down,
):
    tokens_here = residual_in.shape[0]
    local_features = residual_in.shape[1]
    conv_value = (inner_gate.astype(jnp.float32) * conv_input.astype(jnp.float32)).astype(
        jnp.bfloat16
    )
    doc_marks = documents.astype(jnp.bfloat16)
    before_rows, before_docs = from_behind((conv_value[-2:], doc_marks[-2:]), "sp", 1)
    joined_rows = jnp.concatenate([before_rows, conv_value], axis=0).astype(jnp.float32)
    joined_docs = jnp.concatenate([before_docs, doc_marks], axis=0)
    same_one = (joined_docs[1:-1] == doc_marks).astype(jnp.float32)[:, None]
    same_two = (joined_docs[:-2] == doc_marks).astype(jnp.float32)[:, None]
    conv_sum = (
        conv_taps[2] * joined_rows[2:]
        + conv_taps[1] * joined_rows[1:-1] * same_one
        + conv_taps[0] * joined_rows[:-2] * same_two
    )
    mixed = (outer_gate.astype(jnp.float32) * conv_sum).astype(jnp.bfloat16)
    piece_f = gather_directly(mixed, "tp", 1).astype(jnp.float32)
    scaled = (piece_f * mixer_gain).astype(jnp.bfloat16)
    accum = jnp.dot(scaled, output_weight, preferred_element_type=jnp.float32)
    squares = jnp.sum(piece_f * piece_f, axis=1)
    mix_scale = lax.rsqrt(squares / mixer_gain.shape[0] + EPS)
    hidden_state = residual_in.astype(jnp.float32) + accum * mix_scale[:, None]
    feature_total = over_copies(jnp.sum(hidden_state * hidden_state, axis=1), "tp")
    model_width = local_features * lax.axis_size("tp")
    normed = (
        hidden_state * lax.rsqrt(feature_total / model_width + EPS)[:, None] * ffn_gain
    ).astype(jnp.bfloat16)
    experts = lax.axis_size("sp") * expert_gate.shape[0]
    capacity = 4 * tokens_here // experts
    target, owners = slot_tables(routes, experts, capacity)
    padded = jnp.concatenate([normed, jnp.zeros((1, local_features), jnp.bfloat16)], axis=0)
    outgoing = padded[owners].reshape(experts, capacity, local_features)
    slices_in = lax.all_to_all(outgoing, "sp", split_axis=0, concat_axis=0, tiled=True)
    arrived = lax.all_gather(slices_in, "tp", axis=2, tiled=True)
    expert_in = arrived.reshape(-1, model_width)
    gate = jnp.dot(expert_in, expert_gate[0], preferred_element_type=jnp.float32)
    upper = jnp.dot(expert_in, expert_up[0], preferred_element_type=jnp.float32)
    act = (jax.nn.silu(gate) * upper).astype(jnp.bfloat16)
    partial_out = jnp.dot(act, expert_down[0], preferred_element_type=jnp.float32)
    summed = lax.psum_scatter(
        partial_out.astype(jnp.bfloat16), "tp", scatter_dimension=1, tiled=True
    )
    returned = lax.all_to_all(
        summed.reshape(experts, capacity, local_features),
        "sp",
        split_axis=0,
        concat_axis=0,
        tiled=True,
    )
    picked = returned.reshape(experts * capacity, local_features)[target].astype(jnp.float32)
    picked = picked.reshape(tokens_here, 2, local_features)
    routed = jnp.sum(picked * route_weights[:, :, None], axis=1)
    return (hidden_state + routed).astype(jnp.bfloat16)


def solution(mesh):
    placed = (
        P("sp", "tp"),
        P("sp", "tp"),
        P("sp", "tp"),
        P("sp", "tp"),
        P("sp"),
        P(None, "tp"),
        P(),
        P(None, "tp"),
        P("tp"),
        P("sp", None),
        P("sp", None),
        P("sp", None, "tp"),
        P("sp", None, "tp"),
        P("sp", "tp", None),
    )
    return jax.shard_map(
        per_device, mesh=mesh, in_specs=placed, out_specs=P("sp", "tp"), check_vma=False
    )
```

profile of v0, /device:TPU:1, one launch (start us, length us, event | category | flops | bytes accessed | tf_op | source)
XLA Modules:
  0.0 252.4 jit_solution(10328017283454354348)
XLA Ops:
  6.5 0.8 convert_element_type.78
  7.3 0.1 slice.41
  7.4 4.5 %collective-permute-start.1 = (bf16[2]{0:T(256)(128)(2,1)S(1)}, bf16[2]{0:T(256)(128)(2,1)S(1)}, u32[]{:S(2)}, u32[]{:S(2)}) collective-permute-start(bf16[2]{0:T(256)(128)(2,1)S(1)} %slice.41), channel_id=1, source_target_pairs={{0,4},{4,8},{8,12},{12,16},{16,20},{20,24},{24,28},{28,32},{32,36}... | collective-permute-start | bytes 20 | tf_op jit(solution)/shard_map/ppermute | solution.py:12
  11.9 0.9 multiply_convert_fusion.2
  12.8 1.9 collective-permute-start
  14.7 0.8 copy.31
  15.5 0.1 eq.37
  15.7 0.1 eq.33
  15.8 0.7 broadcast_multiply_fusion
  16.5 0.8 slice_bitcast_fusion.2
  17.3 1.2 reduce-window.6
  18.5 0.2 slice_reduce_fusion
  18.8 0.1 copy.30
  18.9 0.1 mul.153
  19.1 0.1 fusion.11
  19.2 0.1 pad_maximum_fusion
  19.3 0.8 compare_convert_fusion.1
  20.1 1.0 fusion.15
  21.1 0.1 copy.28
  21.2 0.7 broadcast_in_dim.8
  21.9 4.2 %all-to-all-start = ((bf16[4,256,128]{1,2,0:T(8,128)(2,1)}), bf16[4,256,128]{1,2,0:T(8,128)(2,1)S(1)}, u32[]{:S(2)}, u32[]{:S(2)}) async-start(bf16[4,256,128]{1,2,0:T(8,128)(2,1)} %broadcast_in_dim.8), calls=%async_computation | async-start | bytes 524288 | tf_op jit(solution)/shard_map/all_to_all | solution.py:23
  26.1 2.4 scatter_custom_fusion
  28.5 3.2 %all-to-all-done = bf16[4,256,128]{1,2,0:T(8,128)(2,1)S(1)} async-done(((bf16[4,256,128]{1,2,0:T(8,128)(2,1)}), bf16[4,256,128]{1,2,0:T(8,128)(2,1)S(1)}, u32[]{:S(2)}, u32[]{:S(2)}) %all-to-all-start) | async-done | bytes 262176 | tf_op jit(solution)/shard_map/all_to_all | solution.py:23
  31.8 0.1 multiply_reduce_fusion.2
  31.9 0.8 fusion.8
  32.7 0.4 multiply_reduce_fusion.1
  33.2 0.6 broadcast_in_dim.9
  33.8 3.2 %all-to-all-start.1 = ((f32[4,1,256]{2,1,0:T(1,128)}), f32[4,1,256]{2,1,0:T(1,128)S(1)}, u32[]{:S(2)}, u32[]{:S(2)}) async-start(f32[4,1,256]{2,1,0:T(1,128)} %broadcast_in_dim.9), calls=%async_computation.1 | async-start | bytes 8192 | tf_op jit(solution)/shard_map/all_to_all | solution.py:23
  37.0 0.0 all-gather.2.cloned.1.call-start
  37.1 4.0 %all-to-all-done.1 = f32[4,1,256]{2,1,0:T(1,128)S(1)} async-done(((f32[4,1,256]{2,1,0:T(1,128)}), f32[4,1,256]{2,1,0:T(1,128)S(1)}, u32[]{:S(2)}, u32[]{:S(2)}) %all-to-all-start.1) | async-done | bytes 4128 | tf_op jit(solution)/shard_map/all_to_all | solution.py:23
  41.2 0.1 multiply_convert_fusion.1
  41.3 4.0 %gather_fusion = bf16[1024,512]{1,0:T(8,128)(2,1)S(1)} fusion(bf16[257,512]{1,0:T(8,128)(2,1)S(1)} %concatenate.11, s32[1024]{0:T(1024)S(1)} %fusion.19), kind=kCustom, calls=%fused_computation | custom fusion | bytes 2101248 | tf_op jit(solution)/shard_map/gather | solution.py:97
  45.3 42.3 %all_to_all.21 = bf16[64,16,512]{2,1,0:T(8,128)(2,1)} all-to-all(bf16[64,16,512]{2,1,0:T(8,128)(2,1)S(1)} %bitcast.54), channel_id=1, replica_groups=mesh['sp'=64,'tp'=4] {'sp'}, dimensions={0} | all-to-all | bytes 2097152 | tf_op jit(solution)/shard_map/all_to_all | solution.py:98
  87.6 0.0 all-gather.2.cloned.1.call-update
  87.7 0.0 reduce-scatter.2.cloned.1.call-start
  87.7 45.8 %all-gather.2.cloned.1.call-done = bf16[64,16,2048]{2,1,0:T(8,128)(2,1)} async-done(((bf16[64,16,512]{2,1,0:T(8,128)(2,1)}), bf16[64,16,2048]{2,1,0:T(8,128)(2,1)}) %all-gather.2.cloned.1.call-update) | async-done | bytes 4194320 | tf_op jit(solution)/shard_map/all_gather | solution.py:99
  133.5 7.5 %fusion.1 = f32[1024,896]{1,0:T(8,128)S(1)} fusion(bf16[1024,2048]{1,0:T(8,128)(2,1)} %bitcast.59, bf16[1,2048,896]{2,1,0:T(8,128)(2,1)} %param.26), kind=kOutput, calls=%fused_computation.5 | convolution fusion | flops 3758096384 | bytes 11534336 | tf_op jit(solution)/shard_map/dot_general | solution.py:102
  141.0 4.8 %multiply_convert_fusion = bf16[1024,896]{1,0:T(8,128)(2,1)S(1)} fusion(f32[1024,896]{1,0:T(8,128)S(1)} %fusion.1, bf16[1024,2048]{1,0:T(8,128)(2,1)S(1)} %bitcast.60, bf16[1,2048,896]{2,1,0:T(8,128)(2,1)S(1)} %copy-done.5), kind=kOutput, calls=%fused_computation.9 | convolution fusion | flops 3763601408 | bytes 13369344 | tf_op jit(solution)/shard_map/dot_general | solution.py:101
  145.9 6.1 %convolution_convert_fusion = bf16[1024,2048]{1,0:T(8,128)(2,1)} fusion(bf16[1024,896]{1,0:T(8,128)(2,1)S(1)} %multiply_convert_fusion, bf16[1,896,2048]{2,1,0:T(8,128)(2,1)S(1)} %copy-done.6), kind=kOutput, calls=%fused_computation.3 | convolution fusion | flops 3760193536 | bytes 9699328 | tf_op jit(solution)/shard_map/dot_general | solution.py:104
  151.9 0.0 reduce-scatter.2.cloned.1.call-update
  151.9 50.0 %reduce-scatter.2.cloned.1.call-done = bf16[1024,512]{1,0:T(8,128)(2,1)} async-done(((bf16[1024,2048]{1,0:T(8,128)(2,1)}), bf16[1024,512]{1,0:T(8,128)(2,1)}) %reduce-scatter.2.cloned.1.call-update) | async-done | bytes 1048592 | tf_op jit(solution)/shard_map/reduce_scatter | solution.py:105
  202.0 10.7 %all-to-all-start.3 = ((bf16[64,16,512]{2,1,0:T(8,128)(2,1)}), bf16[64,16,512]{2,1,0:T(8,128)(2,1)S(1)}, u32[]{:S(2)}, u32[]{:S(2)}) async-start(bf16[64,16,512]{2,1,0:T(8,128)(2,1)} %bitcast.55), calls=%async_computation.4 | async-start | bytes 2097152 | tf_op jit(solution)/shard_map/all_to_all | solution.py:108
  212.7 0.1 copy.34
  212.8 28.0 %all-to-all-done.3 = bf16[64,16,512]{2,1,0:T(8,128)(2,1)S(1)} async-done(((bf16[64,16,512]{2,1,0:T(8,128)(2,1)}), bf16[64,16,512]{2,1,0:T(8,128)(2,1)S(1)}, u32[]{:S(2)}, u32[]{:S(2)}) %all-to-all-start.3) | async-done | bytes 1048608 | tf_op jit(solution)/shard_map/all_to_all | solution.py:108
  240.8 2.0 gather_fusion.1
  242.8 0.7 reshape.90
  243.5 1.3 multiply_reduce_fusion
  244.8 0.8 add_convert_fusion
  (29 shorter events, 0.2 us)
Async XLA Ops:
  6.5 26.2 %copy-start = (bf16[512,512]{1,0:T(8,128)(2,1)S(1)}, bf16[512,512]{1,0:T(8,128)(2,1)}, u32[]{:S(2)}) copy-start(bf16[512,512]{1,0:T(8,128)(2,1)} %param.21) | copy-start | bytes 1572868
  6.5 26.2 %copy-start.1 = (bf16[256,512]{1,0:T(8,128)(2,1)S(1)}, bf16[256,512]{1,0:T(8,128)(2,1)}, u32[]{:S(2)}) copy-start(bf16[256,512]{1,0:T(8,128)(2,1)} %param.14) | copy-start | bytes 786436
  6.5 34.6 %copy-start.2 = (f32[512]{0:T(512)S(1)}, f32[512]{0:T(512)}, u32[]{:S(2)}) copy-start(f32[512]{0:T(512)} %param.22) | copy-start | bytes 6148
  7.4 11.8 %collective-permute-start.1 = (bf16[2]{0:T(256)(128)(2,1)S(1)}, bf16[2]{0:T(256)(128)(2,1)S(1)}, u32[]{:S(2)}, u32[]{:S(2)}) collective-permute-start(bf16[2]{0:T(256)(128)(2,1)S(1)} %slice.41), channel_id=1, source_target_pairs={{0,4},{4,8},{8,12},{12,16},{16,20},{20,24},{24,28},{28,32},{32,36}... | collective-permute-start | bytes 20 | tf_op jit(solution)/shard_map/ppermute | solution.py:12
  12.8 7.3 %collective-permute-start = (bf16[2,128]{1,0:T(2,128)(2,1)S(1)}, bf16[2,128]{1,0:T(2,128)(2,1)S(1)}, u32[]{:S(2)}, u32[]{:S(2)}) collective-permute-start(bf16[2,128]{1,0:T(2,128)(2,1)S(1)} %slice.52), channel_id=1, source_target_pairs={{0,4},{4,8},{8,12},{12,16},{16,20},{20,24},{24,28},{28,32},{32,36}... | collective-permute-start | bytes 1544 | tf_op jit(solution)/shard_map/ppermute | solution.py:12
  21.9 9.9 %all-to-all-start = ((bf16[4,256,128]{1,2,0:T(8,128)(2,1)}), bf16[4,256,128]{1,2,0:T(8,128)(2,1)S(1)}, u32[]{:S(2)}, u32[]{:S(2)}) async-start(bf16[4,256,128]{1,2,0:T(8,128)(2,1)} %broadcast_in_dim.8), calls=%async_computation | async-start | bytes 524288 | tf_op jit(solution)/shard_map/all_to_all | solution.py:23
  33.8 7.4 %all-to-all-start.1 = ((f32[4,1,256]{2,1,0:T(1,128)}), f32[4,1,256]{2,1,0:T(1,128)S(1)}, u32[]{:S(2)}, u32[]{:S(2)}) async-start(f32[4,1,256]{2,1,0:T(1,128)} %broadcast_in_dim.9), calls=%async_computation.1 | async-start | bytes 8192 | tf_op jit(solution)/shard_map/all_to_all | solution.py:23
  37.0 96.5 %all-gather.2.cloned.1.call-start = ((), (), s32[]{:S(2)}) async-start(), calls=%async_computation.5 | async-start | bytes 5242880 | tf_op jit(solution)/shard_map/all_gather | solution.py:99
  87.7 114.3 %reduce-scatter.2.cloned.1.call-start = ((), (), s32[]{:S(2)}) async-start(), calls=%async_computation.6 | async-start | bytes 5242880 | tf_op jit(solution)/shard_map/reduce_scatter | solution.py:105
  133.5 7.5 %copy-start.4 = (bf16[64,16,2048]{2,1,0:T(8,128)(2,1)S(1)}, bf16[64,16,2048]{2,1,0:T(8,128)(2,1)}, u32[]{:S(2)}) copy-start(bf16[64,16,2048]{2,1,0:T(8,128)(2,1)} %all-gather.2.cloned.1.call-done) | copy-start | bytes 12582916
  133.5 7.5 %copy-start.5 = (bf16[1,2048,896]{2,1,0:T(8,128)(2,1)S(1)}, bf16[1,2048,896]{2,1,0:T(8,128)(2,1)}, u32[]{:S(2)}) copy-start(bf16[1,2048,896]{2,1,0:T(8,128)(2,1)} %param.25) | copy-start | bytes 11010052
  141.0 4.8 %copy-start.6 = (bf16[1,896,2048]{2,1,0:T(8,128)(2,1)S(1)}, bf16[1,896,2048]{2,1,0:T(8,128)(2,1)}, u32[]{:S(2)}) copy-start(bf16[1,896,2048]{2,1,0:T(8,128)(2,1)} %param.27) | copy-start | bytes 11010052
  151.9 60.8 %copy-start.3 = (f32[256,2]{0,1:T(2,128)S(1)}, f32[256,2]{0,1:T(2,128)}, u32[]{:S(2)}) copy-start(f32[256,2]{0,1:T(2,128)} %param.24) | copy-start | bytes 6148
  202.0 38.9 %all-to-all-start.3 = ((bf16[64,16,512]{2,1,0:T(8,128)(2,1)}), bf16[64,16,512]{2,1,0:T(8,128)(2,1)S(1)}, u32[]{:S(2)}, u32[]{:S(2)}) async-start(bf16[64,16,512]{2,1,0:T(8,128)(2,1)} %bitcast.55), calls=%async_computation.4 | async-start | bytes 2097152 | tf_op jit(solution)/shard_map/all_to_all | solution.py:108
Sparse Core Ops, SparseCore 0:
  87.8 45.6 all-gather.1
  152.1 49.8 reduce-scatter.1
where the time goes:
time: 253 us; the launch traced here: 252 us
  waiting for transfers between devices  131 us (52%)
  blocking collectives  42.3 us (17%)
  starting transfers between devices  24.6 us (10%)
  matrix products  18.8 us (7%)
  between operations  13.7 us (5%)
  local copies, waits for them, and re-layouts  13.1 us (5%)
  other arithmetic  8.73 us (3%)
    reduce_scatter x1, waiting for transfers between devices, per_device(): lax.psum_scatter(partial_out.astype(jnp.bfloat16), 'tp', scatter_dimensio...  50 us
    all_gather x1, waiting for transfers between devices, per_device(): arrived = lax.all_gather(slices_in, 'tp', axis=2, tiled=True)  45.8 us
    all_to_all x1, blocking collectives, per_device(): lax.all_to_all(outgoing, 'sp', split_axis=0, concat_axis=0, tiled=True)  42.3 us
    all_to_all x1, waiting for transfers between devices, per_device(): lax.all_to_all(summed.reshape(experts, capacity, local_features), 'sp', s...  28 us
    all_to_all x1, starting transfers between devices, per_device(): lax.all_to_all(summed.reshape(experts, capacity, local_features), 'sp', s...  10.7 us
    dot_general x1, matrix products, per_device(): upper = jnp.dot(expert_in, expert_up[0], preferred_element_type=jnp.float32)  7.49 us
    all_to_all x2, starting transfers between devices, sent_to_all(): return lax.all_to_all(copies, axis, split_axis=0, concat_axis=0, tiled=True)  7.43 us
    all_to_all x2, waiting for transfers between devices, sent_to_all(): return lax.all_to_all(copies, axis, split_axis=0, concat_axis=0, tiled=True)  7.29 us
  transfers between devices with their start and end apart: 7, of which 5 were waited for; matrix products, arithmetic and copies ran while one was open for 3% of the time, Pallas kernels for 0%

commit v1 on v0

--- a/solution.py
+++ b/solution.py
@@ -2,8 +2,15 @@
 import jax.numpy as jnp
 from jax import lax
 from jax.sharding import PartitionSpec as P
+from jax.lax import axis_index, axis_size, ppermute
 
 EPS = 1e-06
+
+
+def _advance_views(matrix, in_dim):
+    base_arr = list(matrix.shape[1:])
+    base_arr[in_dim] *= matrix.shape[0]
+    return jnp.moveaxis(matrix, 0, in_dim).reshape(base_arr)
 
 
 def from_behind(block, axis, distance):
@@ -96,7 +103,31 @@
     padded = jnp.concatenate([normed, jnp.zeros((1, local_features), jnp.bfloat16)], axis=0)
     outgoing = padded[owners].reshape(experts, capacity, local_features)
     slices_in = lax.all_to_all(outgoing, "sp", split_axis=0, concat_axis=0, tiled=True)
-    arrived = lax.all_gather(slices_in, "tp", axis=2, tiled=True)
+
+    def drive_files(packet, axis_name, array_axis):
+        how_many = axis_size(axis_name)
+        parts_seen = tuple(((k0, (k0 + 1) % how_many) for k0 in range(how_many)))
+        rack = tuple(((ii, hop_no) for hop_no, ii in parts_seen))
+        d_next, part_next = ([], [])
+        for p in range(how_many - 1):
+            if p % 2 == 0:
+                long_array = ppermute(
+                    d_next[-1] if d_next else packet, axis_name=axis_name, perm=parts_seen
+                )
+                d_next.append(long_array)
+            else:
+                w_next = ppermute(
+                    part_next[-1] if part_next else packet, axis_name=axis_name, perm=rack
+                )
+                part_next.append(w_next)
+        row_out = jnp.stack([*d_next[::-1], packet, *part_next])
+        carry_in = axis_index(axis_name)
+        reply = len(d_next)
+        passed = carry_in - reply
+        row_out = row_out[(jnp.arange(how_many) - passed) % how_many]
+        return _advance_views(row_out, array_axis)
+
+    arrived = drive_files(slices_in, "tp", 2)
     expert_in = arrived.reshape(-1, model_width)
     gate = jnp.dot(expert_in, expert_gate[0], preferred_element_type=jnp.float32)
     upper = jnp.dot(expert_in, expert_up[0], preferred_element_type=jnp.float32)

time: 253 us -> 271 us (1.071)
  local copies, waits for them, and re-layouts: 13.1 us -> 30.6 us
  other arithmetic: 8.73 us -> 12.2 us
  waiting for transfers between devices: 131 us -> 128 us
  matrix products: 18.8 us -> 16 us
    ppermute x0 -> x3, waiting for transfers between devices: none -> 46.1 us  [the longest x2 46.1 us: drive_files(): ppermute(d_next[-1] if d_next else packet, axis_name=axis_name, perm=part...]
    all_gather x1 -> x0, waiting for transfers between devices: 45.8 us -> none  [per_device(): arrived = lax.all_gather(slices_in, 'tp', axis=2, tiled=True)]
    transpose x0 -> x1, local copies, waits for them, and re-layouts: none -> 10.5 us  [_advance_views(): return jnp.moveaxis(matrix, 0, in_dim).reshape(base_arr)]
    gather x0 -> x1, local copies, waits for them, and re-layouts: none -> 4.97 us  [drive_files(): row_out = row_out[(jnp.arange(how_many) - passed) % how_many]]
    another operation x2 -> x3, other arithmetic: 1.24 us -> 4.66 us  [the longest x1 3.42 us: drive_files(): row_out = jnp.stack([*d_next[::-1], packet, *part_next])]
    reduce_scatter x1, waiting for transfers between devices: 50 us -> 46.7 us  [per_device(): lax.psum_scatter(partial_out.astype(jnp.bfloat16), 'tp', scatter_dimensio...]
    dot_general x1, matrix products: 7.49 us -> 4.73 us  [per_device(): upper = jnp.dot(expert_in, expert_up[0], preferred_element_type=jnp.float32)]
  transfers between devices with their start and end apart: 7 -> 9, of which waited for: 5 -> 6; matrix products, arithmetic and copies ran while one was open for 3% -> 3% of each run, Pallas kernels for 0% -> 0%
where the time goes in v1:
time: 271 us; the launch traced here: 270 us
  waiting for transfers between devices  128 us (47%)
  blocking collectives  42.2 us (16%)
  local copies, waits for them, and re-layouts  30.6 us (11%)
  starting transfers between devices  27.3 us (10%)
  matrix products  16 us (6%)
  between operations  13.7 us (5%)
  other arithmetic  12.2 us (5%)
    reduce_scatter x1, waiting for transfers between devices, per_device(): lax.psum_scatter(partial_out.astype(jnp.bfloat16), 'tp', scatter_dimensio...  46.7 us
    ppermute x2, waiting for transfers between devices, drive_files(): ppermute(d_next[-1] if d_next else packet, axis_name=axis_name, perm=part...  46.1 us
    all_to_all x1, blocking collectives, per_device(): lax.all_to_all(outgoing, 'sp', split_axis=0, concat_axis=0, tiled=True)  42.2 us
    all_to_all x1, waiting for transfers between devices, per_device(): lax.all_to_all(summed.reshape(experts, capacity, local_features), 'sp', s...  28 us
    all_to_all x1, starting transfers between devices, per_device(): lax.all_to_all(summed.reshape(experts, capacity, local_features), 'sp', s...  10.7 us
    transpose x1, local copies, waits for them, and re-layouts, _advance_views(): return jnp.moveaxis(matrix, 0, in_dim).reshape(base_arr)  10.5 us
    all_to_all x2, starting transfers between devices, sent_to_all(): return lax.all_to_all(copies, axis, split_axis=0, concat_axis=0, tiled=True)  7.43 us
    all_to_all x2, waiting for transfers between devices, sent_to_all(): return lax.all_to_all(copies, axis, split_axis=0, concat_axis=0, tiled=True)  7.29 us
  transfers between devices with their start and end apart: 9, of which 6 were waited for; matrix products, arithmetic and copies ran while one was open for 3% of the time, Pallas kernels for 0%

profile of v1, /device:TPU:1, one launch (start us, length us, event | category | flops | bytes accessed | tf_op | source)
XLA Modules:
  0.0 270.1 jit_solution(891647064858020380)
XLA Ops:
  6.5 0.8 convert_element_type.78
  7.4 4.5 %collective-permute-start.1 = (bf16[2]{0:T(256)(128)(2,1)S(1)}, bf16[2]{0:T(256)(128)(2,1)S(1)}, u32[]{:S(2)}, u32[]{:S(2)}) collective-permute-start(bf16[2]{0:T(256)(128)(2,1)S(1)} %slice.41), channel_id=1, source_target_pairs={{0,4},{4,8},{8,12},{12,16},{16,20},{20,24},{24,28},{28,32},{32,36}... | collective-permute-start | bytes 20 | tf_op jit(solution)/shard_map/ppermute | solution.py:19
  11.9 0.9 multiply_convert_fusion.2
  12.8 1.9 collective-permute-start
  14.7 0.8 copy.39
  15.5 0.1 eq.39
  15.7 0.1 eq.35
  15.8 0.7 broadcast_multiply_fusion
  16.5 0.8 slice_bitcast_fusion.2
  17.3 1.2 reduce-window.6
  18.5 0.2 slice_reduce_fusion
  18.8 0.1 copy.38
  18.9 0.1 mul.153
  19.1 0.1 fusion.11
  19.3 0.8 compare_convert_fusion.1
  20.1 1.0 fusion.15
  21.2 0.7 broadcast_in_dim.8
  21.9 4.2 %all-to-all-start = ((bf16[4,256,128]{1,2,0:T(8,128)(2,1)}), bf16[4,256,128]{1,2,0:T(8,128)(2,1)S(1)}, u32[]{:S(2)}, u32[]{:S(2)}) async-start(bf16[4,256,128]{1,2,0:T(8,128)(2,1)} %broadcast_in_dim.8), calls=%async_computation | async-start | bytes 524288 | tf_op jit(solution)/shard_map/all_to_all | solution.py:30
  26.1 2.4 scatter_custom_fusion
  28.5 3.2 %all-to-all-done = bf16[4,256,128]{1,2,0:T(8,128)(2,1)S(1)} async-done(((bf16[4,256,128]{1,2,0:T(8,128)(2,1)}), bf16[4,256,128]{1,2,0:T(8,128)(2,1)S(1)}, u32[]{:S(2)}, u32[]{:S(2)}) %all-to-all-start) | async-done | bytes 262176 | tf_op jit(solution)/shard_map/all_to_all | solution.py:30
  31.9 0.8 fusion.8
  32.7 0.4 multiply_reduce_fusion.1
  33.2 0.6 broadcast_in_dim.9
  33.8 3.2 %all-to-all-start.1 = ((f32[4,1,256]{2,1,0:T(1,128)}), f32[4,1,256]{2,1,0:T(1,128)S(1)}, u32[]{:S(2)}, u32[]{:S(2)}) async-start(f32[4,1,256]{2,1,0:T(1,128)} %broadcast_in_dim.9), calls=%async_computation.1 | async-start | bytes 8192 | tf_op jit(solution)/shard_map/all_to_all | solution.py:30
  37.1 4.0 %all-to-all-done.1 = f32[4,1,256]{2,1,0:T(1,128)S(1)} async-done(((f32[4,1,256]{2,1,0:T(1,128)}), f32[4,1,256]{2,1,0:T(1,128)S(1)}, u32[]{:S(2)}, u32[]{:S(2)}) %all-to-all-start.1) | async-done | bytes 4128 | tf_op jit(solution)/shard_map/all_to_all | solution.py:30
  41.2 0.1 multiply_convert_fusion.1
  41.3 4.0 %gather_fusion = bf16[1024,512]{1,0:T(8,128)(2,1)S(1)} fusion(bf16[257,512]{1,0:T(8,128)(2,1)S(1)} %concatenate.11, s32[1024]{0:T(1024)S(1)} %fusion.19), kind=kCustom, calls=%fused_computation | custom fusion | bytes 2101248 | tf_op jit(solution)/shard_map/gather | solution.py:104
  45.3 42.2 %all_to_all.21 = bf16[64,16,512]{2,1,0:T(8,128)(2,1)S(1)} all-to-all(bf16[64,16,512]{2,1,0:T(8,128)(2,1)S(1)} %bitcast.65), channel_id=1, replica_groups=mesh['sp'=64,'tp'=4] {'sp'}, dimensions={0} | all-to-all | bytes 2097152 | tf_op jit(solution)/shard_map/all_to_all | solution.py:105
  87.5 0.3 collective-permute-start.2
  87.8 2.4 collective-permute-start.4
  90.2 22.1 %collective-permute-done.2 = bf16[64,16,512]{2,1,0:T(8,128)(2,1)S(1)} collective-permute-done((bf16[64,16,512]{2,1,0:T(8,128)(2,1)S(1)}, bf16[64,16,512]{2,1,0:T(8,128)(2,1)S(1)}, u32[]{:S(2)}, u32[]{:S(2)}) %collective-permute-start.2) | collective-permute-done | bytes 1048608 | tf_op jit(solution)/shard_map/ppermute | solution.py:114
  112.3 24.0 %collective-permute-done.3 = bf16[64,16,512]{2,1,0:T(8,128)(2,1)} collective-permute-done((bf16[64,16,512]{2,1,0:T(8,128)(2,1)S(1)}, bf16[64,16,512]{2,1,0:T(8,128)(2,1)}, u32[]{:S(2)}, u32[]{:S(2)}) %collective-permute-start.3) | collective-permute-done | bytes 1048608 | tf_op jit(solution)/shard_map/ppermute | solution.py:114
  136.3 3.4 %pad_maximum_fusion = bf16[4,64,16,512]{3,2,1,0:T(8,128)(2,1)} fusion(bf16[1,64,16,512]{3,2,1,0:T(8,128)(2,1)} %bitcast.12, bf16[1,64,16,512]{3,2,1,0:T(8,128)(2,1)S(1)} %bitcast.68, bf16[1,64,16,512]{3,2,1,0:T(8,128)(2,1)S(1)} %bitcast.70, bf16[1,64,16,512]{3,2,1,0:T(8,128)(2,1)} %bitcast.9), kind=kLoop, calls=%fused_computation.4 | loop fusion | flops 6291456 | bytes 8388608 | tf_op jit(solution)/shard_map/stack | solution.py:123
  139.7 5.0 %gather_fusion.1 = bf16[4,64,16,512]{3,2,1,0:T(8,128)(2,1)} fusion(bf16[4,64,16,512]{3,2,1,0:T(8,128)(2,1)} %pad_maximum_fusion, s32[1024]{0:T(1024)S(1)} %pad_clamp_fusion.1), kind=kCustom, calls=%fused_computation.1 | custom fusion | bytes 8388624 | tf_op jit(solution)/shard_map/gather | solution.py:127
  144.7 10.5 %copy.42 = bf16[64,16,4,512]{3,2,1,0:T(4,128)(2,1)S(1)} copy(bf16[64,16,4,512]{3,1,0,2:T(8,128)(2,1)} %bitcast.63) | data formatting | bytes 8388608 | tf_op jit(solution)/shard_map/transpose | solution.py:13
  155.2 1.4 copy.46
  156.7 0.6 copy-done.4
  157.3 4.7 %fusion.1 = f32[1024,896]{1,0:T(8,128)S(1)} fusion(bf16[1024,2048]{1,0:T(8,128)(2,1)S(1)} %bitcast.66, bf16[1,2048,896]{2,1,0:T(8,128)(2,1)S(1)} %copy-done.4), kind=kOutput, calls=%fused_computation.7 | convolution fusion | flops 3758096384 | bytes 11534336 | tf_op jit(solution)/shard_map/dot_general | solution.py:133
  162.0 4.8 %multiply_convert_fusion = bf16[1024,896]{1,0:T(8,128)(2,1)S(1)} fusion(f32[1024,896]{1,0:T(8,128)S(1)} %fusion.1, bf16[1024,2048]{1,0:T(8,128)(2,1)S(1)} %bitcast.67, bf16[1,2048,896]{2,1,0:T(8,128)(2,1)S(1)} %copy-done.5), kind=kOutput, calls=%fused_computation.11 | convolution fusion | flops 3763601408 | bytes 13369344 | tf_op jit(solution)/shard_map/dot_general | solution.py:132
  166.9 6.1 %convolution_convert_fusion = bf16[1024,2048]{1,0:T(8,128)(2,1)} fusion(bf16[1024,896]{1,0:T(8,128)(2,1)S(1)} %multiply_convert_fusion, bf16[1,896,2048]{2,1,0:T(8,128)(2,1)S(1)} %copy-done.6), kind=kOutput, calls=%fused_computation.5 | convolution fusion | flops 3760193536 | bytes 9699328 | tf_op jit(solution)/shard_map/dot_general | solution.py:135
  173.0 46.7 %reduce-scatter.2.cloned.1.call-done = bf16[1024,512]{1,0:T(8,128)(2,1)} async-done(((bf16[1024,2048]{1,0:T(8,128)(2,1)}), bf16[1024,512]{1,0:T(8,128)(2,1)}) %reduce-scatter.2.cloned.1.call-update) | async-done | bytes 1048592 | tf_op jit(solution)/shard_map/reduce_scatter | solution.py:136
  219.7 10.7 %all-to-all-start.3 = ((bf16[64,16,512]{2,1,0:T(8,128)(2,1)}), bf16[64,16,512]{2,1,0:T(8,128)(2,1)S(1)}, u32[]{:S(2)}, u32[]{:S(2)}) async-start(bf16[64,16,512]{2,1,0:T(8,128)(2,1)} %bitcast.69), calls=%async_computation.4 | async-start | bytes 2097152 | tf_op jit(solution)/shard_map/all_to_all | solution.py:139
  230.4 0.1 copy.43
  230.6 28.0 %all-to-all-done.3 = bf16[64,16,512]{2,1,0:T(8,128)(2,1)S(1)} async-done(((bf16[64,16,512]{2,1,0:T(8,128)(2,1)}), bf16[64,16,512]{2,1,0:T(8,128)(2,1)S(1)}, u32[]{:S(2)}, u32[]{:S(2)}) %all-to-all-start.3) | async-done | bytes 1048608 | tf_op jit(solution)/shard_map/all_to_all | solution.py:139
  258.6 2.0 gather_fusion.2
  260.5 0.7 reshape.135
  261.2 1.3 multiply_reduce_fusion
  262.5 0.8 add_convert_fusion
  (38 shorter events, 0.6 us)
Async XLA Ops:
  6.5 26.2 %copy-start = (bf16[512,512]{1,0:T(8,128)(2,1)S(1)}, bf16[512,512]{1,0:T(8,128)(2,1)}, u32[]{:S(2)}) copy-start(bf16[512,512]{1,0:T(8,128)(2,1)} %param.21) | copy-start | bytes 1572868
  6.5 26.2 %copy-start.1 = (bf16[256,512]{1,0:T(8,128)(2,1)S(1)}, bf16[256,512]{1,0:T(8,128)(2,1)}, u32[]{:S(2)}) copy-start(bf16[256,512]{1,0:T(8,128)(2,1)} %param.14) | copy-start | bytes 786436
  6.5 34.6 %copy-start.2 = (f32[512]{0:T(512)S(1)}, f32[512]{0:T(512)}, u32[]{:S(2)}) copy-start(f32[512]{0:T(512)} %param.22) | copy-start | bytes 6148
  7.4 11.8 %collective-permute-start.1 = (bf16[2]{0:T(256)(128)(2,1)S(1)}, bf16[2]{0:T(256)(128)(2,1)S(1)}, u32[]{:S(2)}, u32[]{:S(2)}) collective-permute-start(bf16[2]{0:T(256)(128)(2,1)S(1)} %slice.41), channel_id=1, source_target_pairs={{0,4},{4,8},{8,12},{12,16},{16,20},{20,24},{24,28},{28,32},{32,36}... | collective-permute-start | bytes 20 | tf_op jit(solution)/shard_map/ppermute | solution.py:19
  12.8 7.3 %collective-permute-start = (bf16[2,128]{1,0:T(2,128)(2,1)S(1)}, bf16[2,128]{1,0:T(2,128)(2,1)S(1)}, u32[]{:S(2)}, u32[]{:S(2)}) collective-permute-start(bf16[2,128]{1,0:T(2,128)(2,1)S(1)} %slice.54), channel_id=1, source_target_pairs={{0,4},{4,8},{8,12},{12,16},{16,20},{20,24},{24,28},{28,32},{32,36}... | collective-permute-start | bytes 1544 | tf_op jit(solution)/shard_map/ppermute | solution.py:19
  21.9 9.9 %all-to-all-start = ((bf16[4,256,128]{1,2,0:T(8,128)(2,1)}), bf16[4,256,128]{1,2,0:T(8,128)(2,1)S(1)}, u32[]{:S(2)}, u32[]{:S(2)}) async-start(bf16[4,256,128]{1,2,0:T(8,128)(2,1)} %broadcast_in_dim.8), calls=%async_computation | async-start | bytes 524288 | tf_op jit(solution)/shard_map/all_to_all | solution.py:30
  33.8 7.4 %all-to-all-start.1 = ((f32[4,1,256]{2,1,0:T(1,128)}), f32[4,1,256]{2,1,0:T(1,128)S(1)}, u32[]{:S(2)}, u32[]{:S(2)}) async-start(f32[4,1,256]{2,1,0:T(1,128)} %broadcast_in_dim.9), calls=%async_computation.1 | async-start | bytes 8192 | tf_op jit(solution)/shard_map/all_to_all | solution.py:30
  37.0 182.6 %reduce-scatter.2.cloned.1.call-start = ((), (), s32[]{:S(2)}) async-start(), calls=%async_computation.5 | async-start | bytes 5242880 | tf_op jit(solution)/shard_map/reduce_scatter | solution.py:136
  87.5 24.8 %collective-permute-start.2 = (bf16[64,16,512]{2,1,0:T(8,128)(2,1)S(1)}, bf16[64,16,512]{2,1,0:T(8,128)(2,1)S(1)}, u32[]{:S(2)}, u32[]{:S(2)}) collective-permute-start(bf16[64,16,512]{2,1,0:T(8,128)(2,1)S(1)} %all_to_all.21), channel_id=1, source_target_pairs={{0,1},{1,2},{2,3},{3,0},{4,5},{5,6},{6,7},{7,4},{8,9},{9,10},{10,1... | collective-permute-start | bytes 3145736 | tf_op jit(solution)/shard_map/ppermute | solution.py:114
  87.8 24.5 %collective-permute-start.4 = (bf16[64,16,512]{2,1,0:T(8,128)(2,1)S(1)}, bf16[64,16,512]{2,1,0:T(8,128)(2,1)}, u32[]{:S(2)}, u32[]{:S(2)}) collective-permute-start(bf16[64,16,512]{2,1,0:T(8,128)(2,1)S(1)} %all_to_all.21), channel_id=1, source_target_pairs={{1,0},{2,1},{3,2},{0,3},{5,4},{6,5},{7,6},{4,7},{9,8},{10,9},{11,1... | collective-permute-start | bytes 3145736 | tf_op jit(solution)/shard_map/ppermute | solution.py:119
  112.3 24.0 %collective-permute-start.3 = (bf16[64,16,512]{2,1,0:T(8,128)(2,1)S(1)}, bf16[64,16,512]{2,1,0:T(8,128)(2,1)}, u32[]{:S(2)}, u32[]{:S(2)}) collective-permute-start(bf16[64,16,512]{2,1,0:T(8,128)(2,1)S(1)} %collective-permute-done.2), channel_id=1, source_target_pairs={{0,1},{1,2},{2,3},{3,0},{4,5},{5,6},{6,7},{7,4},{8,9},{9,10},{10,1... | collective-permute-start | bytes 3145736 | tf_op jit(solution)/shard_map/ppermute | solution.py:114
  155.2 2.0 copy-start.4
  157.3 4.7 %copy-start.5 = (bf16[1,2048,896]{2,1,0:T(8,128)(2,1)S(1)}, bf16[1,2048,896]{2,1,0:T(8,128)(2,1)}, u32[]{:S(2)}) copy-start(bf16[1,2048,896]{2,1,0:T(8,128)(2,1)} %param.25) | copy-start | bytes 11010052
  162.0 4.8 %copy-start.6 = (bf16[1,896,2048]{2,1,0:T(8,128)(2,1)S(1)}, bf16[1,896,2048]{2,1,0:T(8,128)(2,1)}, u32[]{:S(2)}) copy-start(bf16[1,896,2048]{2,1,0:T(8,128)(2,1)} %param.27) | copy-start | bytes 11010052
  172.9 57.5 %copy-start.3 = (f32[256,2]{0,1:T(2,128)S(1)}, f32[256,2]{0,1:T(2,128)}, u32[]{:S(2)}) copy-start(f32[256,2]{0,1:T(2,128)} %param.24) | copy-start | bytes 6148
  219.7 38.9 %all-to-all-start.3 = ((bf16[64,16,512]{2,1,0:T(8,128)(2,1)}), bf16[64,16,512]{2,1,0:T(8,128)(2,1)S(1)}, u32[]{:S(2)}, u32[]{:S(2)}) async-start(bf16[64,16,512]{2,1,0:T(8,128)(2,1)} %bitcast.69), calls=%async_computation.4 | async-start | bytes 2097152 | tf_op jit(solution)/shard_map/all_to_all | solution.py:139
Sparse Core Ops, SparseCore 0:
  173.1 46.5 reduce-scatter.1
